TPU v7x, 32 devices: a whole 2x2x4 slice. The times are simulated.
32 devices in a mesh: ep: 8 (over z, x), tp: 4 (over y, core).
Axes of the slice: x: 2, y: 2, z: 4, core: 2. Of those that a mesh axis runs over, the one named last changes fastest.
Arguments:
- tokens: bfloat16 [1024, 2048], P('ep'), may hold values from -6 to 6
- routing: int32 [1024, 2], P('ep'), may hold values from 0 to 7, all different within a row; in each aligned block of 128 rows (0 to 127, 128 to 255, ...) at most 56 rows name the same one
- router_weight: bfloat16 [2048, 8], replicated, may hold values from -0.125 to 0.125
- gate_weight: bfloat16 [8, 2048, 2048], P('ep', None, 'tp'), may hold values from -0.125 to 0.125
- up_weight: bfloat16 [8, 2048, 2048], P('ep', None, 'tp'), may hold values from -0.125 to 0.125
- down_weight: bfloat16 [8, 2048, 2048], P('ep', 'tp'), may hold values from -0.125 to 0.125
- cotangent: bfloat16 [1024, 2048], P('ep'), may hold values from -0.796875 to 0.796875
Outputs:
- token_grad: bfloat16 [1024, 2048], P('ep')
- router_grad: float32 [2048, 8], P('tp')
- router_rows: float32 [2048], P('tp')
- gate_grad: bfloat16 [8, 2048, 2048], P('ep', None, 'tp')
- up_grad: bfloat16 [8, 2048, 2048], P('ep', None, 'tp')
- down_grad: bfloat16 [8, 2048, 2048], P('ep', 'tp')
- gate_rows: float32 [8, 2048], P('ep')
- up_rows: float32 [8, 2048], P('ep')
- down_rows: float32 [8, 2048], P('ep', 'tp')
Inputs may be any that keep to these rules, and one draw needn't show every extreme that they name: `routing`: A row's 2 experts differ. Within the rows of one index of ep (128 rows), no expert is named more than 56 times, a bound that some block reaches.
All inputs are finite; a program needn't handle non-finite values.
Results may differ from a plain program's by a relative error of at most 0.01.
Values may be sent and summed in bfloat16 or wider, within the bound.
A program may use at most 64 MiB of HBM per device.

v0:
```python
import jax
import jax.numpy as jnp
from jax import lax
from jax.sharding import PartitionSpec as P


def expert_backward(rows_in, cots_in, slot_scale, w_gate, w_up, w_down):
    pre_gate = jnp.dot(rows_in, w_gate, preferred_element_type=jnp.float32)
    pre_up = jnp.dot(rows_in, w_up, preferred_element_type=jnp.float32)
    sigmoid_gate = jax.nn.sigmoid(pre_gate)
    hidden = (pre_gate * sigmoid_gate * pre_up).astype(jnp.bfloat16)
    back_proj = lax.dot_general(
        cots_in, w_down, (((1,), (1,)), ((), ())), preferred_element_type=jnp.float32
    )
    gate_term = jnp.sum(hidden.astype(jnp.float32) * back_proj, axis=1)
    scaled = slot_scale * back_proj
    grad_up_pre = (scaled * pre_gate * sigmoid_gate).astype(jnp.bfloat16)
    grad_gate_pre = (
        scaled * pre_up * sigmoid_gate * (1.0 + pre_gate * (1.0 - sigmoid_gate))
    ).astype(jnp.bfloat16)
    weighted = (slot_scale * cots_in.astype(jnp.float32)).astype(jnp.bfloat16)
    contract_rows = (((0,), (0,)), ((), ()))
    grad_down = lax.dot_general(hidden, weighted, contract_rows, preferred_element_type=jnp.float32)
    grad_gate = lax.dot_general(
        rows_in, grad_gate_pre, contract_rows, preferred_element_type=jnp.float32
    )
    grad_up = lax.dot_general(
        rows_in, grad_up_pre, contract_rows, preferred_element_type=jnp.float32
    )
    contract_hidden = (((1,), (1,)), ((), ()))
    partial_value = lax.dot_general(
        grad_gate_pre, w_gate, contract_hidden, preferred_element_type=jnp.float32
    )
    partial_value = partial_value + lax.dot_general(
        grad_up_pre, w_up, contract_hidden, preferred_element_type=jnp.float32
    )
    return (partial_value, gate_term, grad_gate, grad_up, grad_down)


def per_device(tokens, routing, router_weight, gate_weight, up_weight, down_weight, cotangent):
    groups = lax.axis_size("ep")
    shares = lax.axis_size("tp")
    tok_count, model_width = tokens.shape
    top_count = routing.shape[1]
    local_experts = gate_weight.shape[0]
    experts = local_experts * groups
    capacity = 7 * tok_count * top_count // (4 * experts)
    slot_span = groups * capacity
    assigns = tok_count * top_count
    col_width = model_width // shares
    col_start = lax.axis_index("tp") * col_width
    logits = jnp.dot(tokens, router_weight, preferred_element_type=jnp.float32)
    affinity = jax.nn.sigmoid(logits)
    chosen = jnp.take_along_axis(affinity, routing, axis=1)
    total_aff = jnp.sum(chosen, axis=1, keepdims=True)
    weights = chosen / total_aff
    flat_ids = routing.reshape(-1)
    onehot_ids = (flat_ids[:, None] == jnp.arange(experts, dtype=jnp.int32)[None, :]).astype(
        jnp.int32
    )
    position = jnp.sum((jnp.cumsum(onehot_ids, axis=0) - 1) * onehot_ids, axis=1)
    slot_of = flat_ids % local_experts * slot_span + flat_ids // local_experts * capacity + position
    slot_table = jnp.full((local_experts * slot_span,), assigns, jnp.int32)
    slot_table = slot_table.at[slot_of].set(jnp.arange(assigns, dtype=jnp.int32))
    zero_row = jnp.zeros((1, model_width), jnp.bfloat16)
    tok_pad = jnp.concatenate([tokens, zero_row], axis=0)
    cot_pad = jnp.concatenate([cotangent, zero_row], axis=0)
    weight_pad = jnp.concatenate(
        [weights.astype(jnp.bfloat16).reshape(-1), jnp.zeros((1,), jnp.bfloat16)]
    )
    source_tok = slot_table // top_count
    rows_send = tok_pad[source_tok].reshape(local_experts, groups, capacity, model_width)
    cots_send = cot_pad[source_tok].reshape(local_experts, groups, capacity, model_width)
    scale_send = weight_pad[slot_table].reshape(local_experts, groups, capacity)
    rows_recv, cots_recv, scale_recv = (
        lax.all_to_all(rows_send, "ep", split_axis=1, concat_axis=1, tiled=True),
        lax.all_to_all(cots_send, "ep", split_axis=1, concat_axis=1, tiled=True),
        lax.all_to_all(scale_send, "ep", split_axis=1, concat_axis=1, tiled=True),
    )
    partials, gate_terms, gate_grads, up_grads, down_grads = ([], [], [], [], [])
    slot_scale = scale_recv[0].reshape(slot_span).astype(jnp.float32)[:, None]
    result = expert_backward(
        rows_recv[0].reshape(slot_span, model_width),
        cots_recv[0].reshape(slot_span, model_width),
        slot_scale,
        gate_weight[0],
        up_weight[0],
        down_weight[0],
    )
    partials.append(result[0])
    gate_terms.append(result[1])
    gate_grads.append(result[2])
    up_grads.append(result[3])
    down_grads.append(result[4])
    partial_value = jnp.stack(partials)
    gate_term = jnp.stack(gate_terms)
    grad_gate = jnp.stack(gate_grads)
    grad_up = jnp.stack(up_grads)
    grad_down = jnp.stack(down_grads)
    gate_rows, up_rows = lax.psum(
        (jnp.sum(grad_gate * grad_gate, axis=2), jnp.sum(grad_up * grad_up, axis=2)), "tp"
    )
    down_rows = jnp.sum(grad_down * grad_down, axis=2)
    summed = lax.psum_scatter(partial_value, "tp", scatter_dimension=2, tiled=True)
    gate_sum = lax.psum(gate_term, "tp")
    back_send = summed.astype(jnp.bfloat16).reshape(local_experts, groups, capacity, col_width)
    gate_send = gate_sum.astype(jnp.bfloat16).reshape(local_experts, groups, capacity)
    back_recv, gate_recv = (
        lax.all_to_all(back_send, "ep", split_axis=1, concat_axis=1, tiled=True),
        lax.all_to_all(gate_send, "ep", split_axis=1, concat_axis=1, tiled=True),
    )
    router_cols = lax.dynamic_slice_in_dim(router_weight, col_start, col_width, 0)
    back_flat = back_recv.reshape(local_experts * slot_span, -1)
    back_rows = jnp.sum(
        back_flat[slot_of].astype(jnp.float32).reshape(tok_count, top_count, -1), axis=1
    )
    d_weights = gate_recv.reshape(-1)[slot_of].astype(jnp.float32).reshape(tok_count, top_count)
    d_chosen = (d_weights - jnp.sum(d_weights * weights, axis=1, keepdims=True)) / total_aff
    d_logit = d_chosen * chosen * (1.0 - chosen)
    onehot = (routing[:, :, None] == jnp.arange(experts, dtype=jnp.int32)[None, None, :]).astype(
        jnp.float32
    )
    d_logits = jnp.sum(d_logit[:, :, None] * onehot, axis=1).astype(jnp.bfloat16)
    token_cols = lax.dynamic_slice_in_dim(tokens, col_start, col_width, 1)
    router_part = lax.dot_general(
        token_cols, d_logits, (((0,), (0,)), ((), ())), preferred_element_type=jnp.float32
    )
    router_grad = lax.psum(router_part, "ep")
    router_rows = jnp.sum(router_grad * router_grad, axis=1)
    router_back = lax.dot_general(
        d_logits, router_cols, (((1,), (1,)), ((), ())), preferred_element_type=jnp.float32
    )
    token_grad = (back_rows + router_back).astype(jnp.bfloat16)
    token_grad = lax.all_gather(token_grad, "tp", axis=1, tiled=True)
    return (
        token_grad,
        router_grad,
        router_rows,
        grad_gate.astype(jnp.bfloat16),
        grad_up.astype(jnp.bfloat16),
        grad_down.astype(jnp.bfloat16),
        gate_rows,
        up_rows,
        down_rows,
    )


def solution(mesh):
    return jax.shard_map(
        per_device,
        mesh=mesh,
        in_specs=(
            P("ep", None),
            P("ep", None),
            P(),
            P("ep", None, "tp"),
            P("ep", None, "tp"),
            P("ep", "tp", None),
            P("ep", None),
        ),
        out_specs=(
            P("ep", None),
            P("tp", None),
            P("tp"),
            P("ep", None, "tp"),
            P("ep", None, "tp"),
            P("ep", "tp", None),
            P("ep", None),
            P("ep", None),
            P("ep", "tp"),
        ),
        check_vma=False,
    )
```

profile of v0, /device:TPU:0, one launch (start us, length us, event | category | flops | bytes accessed | tf_op | source)
XLA Modules:
  0.0 255.0 jit_solution(7731860463774829727)
XLA Ops:
  7.2 0.8 broadcast_multiply_fusion
  8.0 0.8 copy.81
  9.1 0.7 bitcast_or_fusion
  10.0 0.6 reduce-window.6
  10.6 0.2 slice_reduce_fusion
  11.0 1.4 scatter_custom_fusion
  12.7 1.3 fusion.14
  14.0 1.4 gather_fusion.5
  15.6 0.6 fusion.29
  16.4 0.1 convert_element_type.88
  16.6 3.2 %gather_fusion = bf16[448]{0:T(512)(128)(2,1)S(1)} fusion(bf16[257]{0:T(512)(128)(2,1)S(1)} %pad_maximum_fusion, s32[1024]{0:T(1024)S(1)} %get-tuple-element.83), kind=kCustom, calls=%fused_computation | custom fusion | bytes 3584 | tf_op jit(solution)/shard_map/gather | solution.py:74
  19.7 0.7 reshape.229
  20.4 7.3 %all-to-all-start = ((bf16[1,8,56]{2,0,1:T(2,128)(2,1)}), bf16[1,8,56]{2,0,1:T(2,128)(2,1)S(1)}, u32[]{:S(2)}, u32[]{:S(2)}) async-start(bf16[1,8,56]{2,0,1:T(2,128)(2,1)} %reshape.229), calls=%async_computation | async-start | bytes 8192 | tf_op jit(solution)/shard_map/all_to_all | solution.py:78
  27.7 3.2 %gather_fusion.2 = bf16[448,2048]{1,0:T(8,128)(2,1)} fusion(bf16[129,2048]{1,0:T(8,128)(2,1)S(1)} %concatenate.11, s32[1024]{0:T(1024)S(1)} %get-tuple-element.82), kind=kCustom, calls=%fused_computation.2 | custom fusion | bytes 3671808 | tf_op jit(solution)/shard_map/gather | solution.py:72
  30.9 3.2 %all-to-all-done = bf16[1,8,56]{2,0,1:T(2,128)(2,1)S(1)} async-done(((bf16[1,8,56]{2,0,1:T(2,128)(2,1)}), bf16[1,8,56]{2,0,1:T(2,128)(2,1)S(1)}, u32[]{:S(2)}, u32[]{:S(2)}) %all-to-all-start) | async-done | bytes 928 | tf_op jit(solution)/shard_map/all_to_all | solution.py:78
  34.1 4.3 %all-to-all-start.2 = ((bf16[1,8,56,2048]{3,2,0,1:T(8,128)(2,1)}), bf16[1,8,56,2048]{3,2,0,1:T(8,128)(2,1)}, u32[]{:S(2)}, u32[]{:S(2)}) async-start(bf16[1,8,56,2048]{3,2,0,1:T(8,128)(2,1)} %bitcast.67), calls=%async_computation.2 | async-start | bytes 3670016 | tf_op jit(solution)/shard_map/all_to_all | solution.py:76
  38.4 1.1 concatenate.10
  39.5 3.2 %gather_fusion.1 = bf16[448,2048]{1,0:T(8,128)(2,1)} fusion(bf16[129,2048]{1,0:T(8,128)(2,1)S(1)} %concatenate.10, s32[1024]{0:T(1024)S(1)} %get-tuple-element.82), kind=kCustom, calls=%fused_computation.1 | custom fusion | bytes 3671808 | tf_op jit(solution)/shard_map/gather | solution.py:73
  42.7 37.2 %all-to-all-done.2 = bf16[1,8,56,2048]{3,2,0,1:T(8,128)(2,1)} async-done(((bf16[1,8,56,2048]{3,2,0,1:T(8,128)(2,1)}), bf16[1,8,56,2048]{3,2,0,1:T(8,128)(2,1)}, u32[]{:S(2)}, u32[]{:S(2)}) %all-to-all-start.2) | async-done | bytes 1835040 | tf_op jit(solution)/shard_map/all_to_all | solution.py:76
  79.9 4.3 %all-to-all-start.1 = ((bf16[1,8,56,2048]{3,2,0,1:T(8,128)(2,1)}), bf16[1,8,56,2048]{3,2,0,1:T(8,128)(2,1)}, u32[]{:S(2)}, u32[]{:S(2)}) async-start(bf16[1,8,56,2048]{3,2,0,1:T(8,128)(2,1)} %bitcast.66), calls=%async_computation.1 | async-start | bytes 3670016 | tf_op jit(solution)/shard_map/all_to_all | solution.py:77
  84.2 0.2 reduce-scatter.2.cloned.1.call-start
  84.6 4.2 %fusion.5 = f32[448,512]{1,0:T(8,128)} fusion(bf16[448,2048]{1,0:T(8,128)(2,1)} %bitcast.11, bf16[1,2048,512]{2,1,0:T(8,128)(2,1)} %param.11), kind=kOutput, calls=%fused_computation.17 | convolution fusion | flops 939524096 | bytes 4849664 | tf_op jit(solution)/shard_map/dot_general | solution.py:9
  88.8 3.5 %fusion.2 = f32[448,512]{1,0:T(8,128)} fusion(bf16[448,2048]{1,0:T(8,128)(2,1)} %bitcast.11, bf16[1,2048,512]{2,1,0:T(8,128)(2,1)S(1)} %copy-done), kind=kOutput, calls=%fused_computation.14 | convolution fusion | flops 939524096 | bytes 4849664 | tf_op jit(solution)/shard_map/dot_general | solution.py:8
  92.3 34.1 %all-to-all-done.1 = bf16[1,8,56,2048]{3,2,0,1:T(8,128)(2,1)} async-done(((bf16[1,8,56,2048]{3,2,0,1:T(8,128)(2,1)}), bf16[1,8,56,2048]{3,2,0,1:T(8,128)(2,1)}, u32[]{:S(2)}, u32[]{:S(2)}) %all-to-all-start.1) | async-done | bytes 1835040 | tf_op jit(solution)/shard_map/all_to_all | solution.py:77
  126.4 5.5 %multiply_reduce_fusion.3 = (f32[448]{0:T(512)}, bf16[448,512]{1,0:T(8,128)(2,1)}, bf16[448,512]{1,0:T(8,128)(2,1)S(1)}, bf16[448,512]{1,0:T(8,128)(2,1)S(1)}) fusion(f32[448,512]{1,0:T(8,128)} %fusion.5, f32[448,512]{1,0:T(8,128)} %fusion.2, f32[448]{0:T(512)S(1)} %reshape.164, bf16[448,2048]{1,0:T(8,128)(2,1)} %bitcast.7, bf16[1,512,2048]{2,1,0:T(8,128)(2,1)} %param.12), kind=kOutput, calls=%fused_computation.32 | convolution fusion | flops 944111168 | bytes 7147008 | tf_op jit(solution)/shard_map/dot_general | solution.py:12
  131.9 1.1 fusion
  133.1 0.4 copy-done.2
  133.5 3.0 %add_bitcast_fusion = f32[1,448,2048]{2,1,0:T(8,128)} fusion(f32[448,2048]{1,0:T(8,128)S(1)} %fusion, bf16[448,512]{1,0:T(8,128)(2,1)S(1)} %get-tuple-element.79, bf16[1,2048,512]{2,1,0:T(8,128)(2,1)S(1)} %copy-done.2), kind=kOutput, calls=%fused_computation.11 | convolution fusion | flops 940441600 | bytes 9895936 | tf_op jit(solution)/shard_map/dot_general | solution.py:34
  136.6 4.1 %convert_bitcast_fusion.2 = (bf16[1,2048,512]{1,2,0:T(8,128)(2,1)}, f32[2048]{0:T(1024)S(1)}) fusion(bf16[448,2048]{1,0:T(8,128)(2,1)} %bitcast.11, bf16[448,512]{1,0:T(8,128)(2,1)S(1)} %get-tuple-element.78), kind=kOutput, calls=%fused_computation.23 | convolution fusion | flops 942667776 | bytes 4399104 | tf_op jit(solution)/shard_map/dot_general | solution.py:24
  140.7 4.3 %convert_bitcast_fusion.1 = (bf16[1,2048,512]{1,2,0:T(8,128)(2,1)}, f32[2048]{0:T(1024)S(1)}) fusion(bf16[448,2048]{1,0:T(8,128)(2,1)} %bitcast.11, bf16[448,512]{1,0:T(8,128)(2,1)S(1)} %get-tuple-element.79), kind=kOutput, calls=%fused_computation.22 | convolution fusion | flops 942667776 | bytes 4399104 | tf_op jit(solution)/shard_map/dot_general | solution.py:27
  145.0 11.0 %all-reduce.2 = (bf16[1,448]{1,0:T(2,128)(2,1)S(1)}, f32[1,2048]{1,0:T(1,128)}, f32[1,2048]{1,0:T(1,128)}) all-reduce(f32[1,448]{1,0:T(1,128)S(1)} %bitcast.73, f32[1,2048]{1,0:T(1,128)S(1)} %bitcast.68, f32[1,2048]{1,0:T(1,128)S(1)} %bitcast.69), channel_id=1, replica_groups=mesh['ep'=8,'tp'=4] {'tp'}, use_global_device_ids=true, to_apply=%region_8.9 | all-reduce | flops 4544 | bytes 35456 | tf_op jit(solution)/shard_map/psum | solution.py:105
  156.0 0.7 reshape.230
  156.7 4.5 %all-to-all-start.4 = ((bf16[1,8,56]{2,0,1:T(2,128)(2,1)}), bf16[1,8,56]{2,0,1:T(2,128)(2,1)S(1)}, u32[]{:S(2)}, u32[]{:S(2)}) async-start(bf16[1,8,56]{2,0,1:T(2,128)(2,1)} %reshape.230), calls=%async_computation.5 | async-start | bytes 8192 | tf_op jit(solution)/shard_map/all_to_all | solution.py:110
  161.3 15.6 %reduce-scatter.2.cloned.1.call-done = f32[1,448,512]{2,1,0:T(8,128)} async-done(((f32[1,448,2048]{2,1,0:T(8,128)}), f32[1,448,512]{2,1,0:T(8,128)}) %reduce-scatter.2.cloned.1.call-update) | async-done | bytes 917520 | tf_op jit(solution)/shard_map/reduce_scatter | solution.py:104
  176.9 2.0 convert_element_type.94
  178.9 5.5 %all-to-all-start.3 = ((bf16[1,8,56,512]{3,2,0,1:T(8,128)(2,1)}), bf16[1,8,56,512]{3,2,0,1:T(8,128)(2,1)S(1)}, u32[]{:S(2)}, u32[]{:S(2)}) async-start(bf16[1,8,56,512]{3,2,0,1:T(8,128)(2,1)} %bitcast.16), calls=%async_computation.4 | async-start | bytes 917504 | tf_op jit(solution)/shard_map/all_to_all | solution.py:109
  184.4 4.9 %multiply_reduce_fusion = (f32[512]{0:T(512)}, bf16[1,512,2048]{2,1,0:T(8,128)(2,1)}) fusion(bf16[448,512]{1,0:T(8,128)(2,1)} %get-tuple-element.67, bf16[448,2048]{1,0:T(8,128)(2,1)} %bitcast.7, f32[448]{0:T(512)S(1)} %copy-done.11), kind=kOutput, calls=%fused_computation.7 | convolution fusion | flops 945421824 | bytes 4394752 | tf_op jit(solution)/shard_map/dot_general | solution.py:23
  189.3 3.9 %copy.90 = bf16[1,2048,512]{2,1,0:T(8,128)(2,1)} copy(bf16[1,2048,512]{1,2,0:T(8,128)(2,1)} %get-tuple-element.76) | data formatting | bytes 4194304
  193.3 3.9 %copy.91 = bf16[1,2048,512]{2,1,0:T(8,128)(2,1)} copy(bf16[1,2048,512]{1,2,0:T(8,128)(2,1)} %get-tuple-element.74) | data formatting | bytes 4194304
  197.3 1.9 gather_fusion.4
  199.7 37.5 %psum.29 = f32[512,8]{0,1:T(8,128)S(1)} all-reduce(f32[512,8]{0,1:T(8,128)S(1)} %fusion.15), channel_id=1, replica_groups=mesh['ep'=8,'tp'=4] {'ep'}, use_global_device_ids=true, to_apply=%region_11.12 | all-reduce | flops 4096 | bytes 32768 | tf_op jit(solution)/shard_map/psum | solution.py:128
  237.2 0.6 multiply_reduce_fusion.4
  237.8 1.2 gather_fusion.3
  239.0 0.3 reshape.165
  239.3 0.6 reduce_sum.101
  239.9 0.9 fusion.11
  240.9 6.5 %all_gather.3 = bf16[128,2048]{1,0:T(8,128)(2,1)S(1)} all-gather(bf16[128,512]{1,0:T(8,128)(2,1)S(1)} %fusion.11), channel_id=1, replica_groups=mesh['ep'=8,'tp'=4] {'tp'}, dimensions={1}, use_global_device_ids=true | all-gather | bytes 655360 | tf_op jit(solution)/shard_map/all_gather | solution.py:134
  247.4 0.8 copy.93
  (60 shorter events, 2.1 us)
Async XLA Ops:
  7.2 81.6 %copy-start = (bf16[1,2048,512]{2,1,0:T(8,128)(2,1)S(1)}, bf16[1,2048,512]{2,1,0:T(8,128)(2,1)}, u32[]{:S(2)}) copy-start(bf16[1,2048,512]{2,1,0:T(8,128)(2,1)} %param.10) | copy-start | bytes 6291460
  11.0 1.7 copy-start.7
  14.0 1.6 copy-start.4
  14.0 13.7 %copy-start.1 = (bf16[128,2048]{1,0:T(8,128)(2,1)S(1)}, bf16[128,2048]{1,0:T(8,128)(2,1)}, u32[]{:S(2)}) copy-start(bf16[128,2048]{1,0:T(8,128)(2,1)} %param.7) | copy-start | bytes 1572868
  15.6 15.3 %copy-start.5 = (f32[128]{0:T(128)}, f32[128]{0:T(128)S(1)}, u32[]{:S(2)}) copy-start(f32[128]{0:T(128)S(1)} %get-tuple-element.70) | copy-start | bytes 1540
  20.4 13.7 %all-to-all-start = ((bf16[1,8,56]{2,0,1:T(2,128)(2,1)}), bf16[1,8,56]{2,0,1:T(2,128)(2,1)S(1)}, u32[]{:S(2)}, u32[]{:S(2)}) async-start(bf16[1,8,56]{2,0,1:T(2,128)(2,1)} %reshape.229), calls=%async_computation | async-start | bytes 8192 | tf_op jit(solution)/shard_map/all_to_all | solution.py:78
  34.1 45.8 %all-to-all-start.2 = ((bf16[1,8,56,2048]{3,2,0,1:T(8,128)(2,1)}), bf16[1,8,56,2048]{3,2,0,1:T(8,128)(2,1)}, u32[]{:S(2)}, u32[]{:S(2)}) async-start(bf16[1,8,56,2048]{3,2,0,1:T(8,128)(2,1)} %bitcast.67), calls=%async_computation.2 | async-start | bytes 3670016 | tf_op jit(solution)/shard_map/all_to_all | solution.py:76
  79.9 46.5 %all-to-all-start.1 = ((bf16[1,8,56,2048]{3,2,0,1:T(8,128)(2,1)}), bf16[1,8,56,2048]{3,2,0,1:T(8,128)(2,1)}, u32[]{:S(2)}, u32[]{:S(2)}) async-start(bf16[1,8,56,2048]{3,2,0,1:T(8,128)(2,1)} %bitcast.66), calls=%async_computation.1 | async-start | bytes 3670016 | tf_op jit(solution)/shard_map/all_to_all | solution.py:77
  84.2 92.7 %reduce-scatter.2.cloned.1.call-start = ((), (), s32[]{:S(2)}) async-start(), calls=%async_computation.6 | async-start | bytes 4587520 | tf_op jit(solution)/shard_map/reduce_scatter | solution.py:104
  84.6 41.8 %copy-start.10 = (f32[448]{0:T(512)}, f32[448]{0:T(512)S(1)}, u32[]{:S(2)}) copy-start(f32[448]{0:T(512)S(1)} %reshape.164) | copy-start | bytes 5380
  131.9 1.6 copy-start.2
  140.7 4.3 %copy-start.12 = (f32[448]{0:T(512)S(1)}, f32[448]{0:T(512)}, u32[]{:S(2)}) copy-start(f32[448]{0:T(512)} %get-tuple-element.66) | copy-start | bytes 5380
  140.7 20.6 %copy-start.8 = (s32[256,1]{0,1:T(1,128)S(1)}, s32[256,1]{0,1:T(1,128)}, u32[]{:S(2)}) copy-start(s32[256,1]{0,1:T(1,128)} %copy-done.7) | copy-start | bytes 3076
  145.0 39.4 %copy-start.11 = (f32[448]{0:T(512)S(1)}, f32[448]{0:T(512)}, u32[]{:S(2)}) copy-start(f32[448]{0:T(512)} %copy-done.10) | copy-start | bytes 5380
  156.7 22.2 %all-to-all-start.4 = ((bf16[1,8,56]{2,0,1:T(2,128)(2,1)}), bf16[1,8,56]{2,0,1:T(2,128)(2,1)S(1)}, u32[]{:S(2)}, u32[]{:S(2)}) async-start(bf16[1,8,56]{2,0,1:T(2,128)(2,1)} %reshape.230), calls=%async_computation.5 | async-start | bytes 8192 | tf_op jit(solution)/shard_map/all_to_all | solution.py:110
  178.9 58.9 %all-to-all-start.3 = ((bf16[1,8,56,512]{3,2,0,1:T(8,128)(2,1)}), bf16[1,8,56,512]{3,2,0,1:T(8,128)(2,1)S(1)}, u32[]{:S(2)}, u32[]{:S(2)}) async-start(bf16[1,8,56,512]{3,2,0,1:T(8,128)(2,1)} %bitcast.16), calls=%async_computation.4 | async-start | bytes 917504 | tf_op jit(solution)/shard_map/all_to_all | solution.py:109
  193.3 6.2 %copy-start.9 = (f32[128,2]{0,1:T(2,128)S(1)}, f32[128,2]{0,1:T(2,128)}, u32[]{:S(2)}) copy-start(f32[128,2]{0,1:T(2,128)} %get-tuple-element.69) | copy-start | bytes 3076
  193.3 6.2 %copy-start.6 = (f32[128]{0:T(128)S(1)}, f32[128]{0:T(128)}, u32[]{:S(2)}) copy-start(f32[128]{0:T(128)} %copy-done.5) | copy-start | bytes 1540
  237.2 3.7 %copy-start.3 = (f32[512,8]{0,1:T(8,128)}, f32[512,8]{0,1:T(8,128)S(1)}, u32[]{:S(2)}) copy-start(f32[512,8]{0,1:T(8,128)S(1)} %psum.29) | copy-start | bytes 49156
Sparse Core Ops, SparseCore 0:
  136.7 40.1 reduce-scatter.1
where the time goes:
time: 256 us; the launch traced here: 255 us
  waiting for transfers between devices  90.1 us (35%)
  blocking collectives  55 us (21%)
  matrix products  33.1 us (13%)
  local copies, waits for them, and re-layouts  30 us (12%)
  starting transfers between devices  26.2 us (10%)
  between operations  14.3 us (6%)
  other arithmetic  6.23 us (2%)
    psum x1, blocking collectives, per_device(): router_grad = lax.psum(router_part, 'ep')  37.5 us
    all_to_all x1, waiting for transfers between devices, per_device(): lax.all_to_all(rows_send, 'ep', split_axis=1, concat_axis=1, tiled=True)  37.2 us
    all_to_all x1, waiting for transfers between devices, per_device(): lax.all_to_all(cots_send, 'ep', split_axis=1, concat_axis=1, tiled=True)  34.1 us
    reduce_scatter x1, waiting for transfers between devices, per_device(): lax.psum_scatter(partial_value, 'tp', scatter_dimension=2, tiled=True)  15.6 us
    psum x1, blocking collectives, per_device(): gate_sum = lax.psum(gate_term, 'tp')  11 us
    unnamed x30, local copies, waits for them, and re-layouts  9.92 us
    all_to_all x1, starting transfers between devices, per_device(): lax.all_to_all(scale_send, 'ep', split_axis=1, concat_axis=1, tiled=True)  7.28 us
    all_gather x1, blocking collectives, per_device(): token_grad = lax.all_gather(token_grad, 'tp', axis=1, tiled=True)  6.5 us
  transfers between devices with their start and end apart: 6, of which 4 were waited for; matrix products, arithmetic and copies ran while one was open for 17% of the time, Pallas kernels for 0%

commit v1 on v0

--- a/solution.py
+++ b/solution.py
@@ -125,7 +125,11 @@
     router_part = lax.dot_general(
         token_cols, d_logits, (((0,), (0,)), ((), ())), preferred_element_type=jnp.float32
     )
-    router_grad = lax.psum(router_part, "ep")
+    router_grad = router_part
+    for hop in (1, 2, 4):
+        router_grad = router_grad + lax.ppermute(
+            router_grad, "ep", [(dev, dev ^ hop) for dev in range(8)]
+        )
     router_rows = jnp.sum(router_grad * router_grad, axis=1)
     router_back = lax.dot_general(
         d_logits, router_cols, (((1,), (1,)), ((), ())), preferred_element_type=jnp.float32

time: 256 us -> 229 us (0.89)
  blocking collectives: 55 us -> 17.5 us
  waiting for transfers between devices: 90.1 us -> 95.8 us
  starting transfers between devices: 26.2 us -> 30.3 us
    psum x1 -> x0, blocking collectives: 37.5 us -> none  [per_device(): router_grad = lax.psum(router_part, 'ep')]
    reduce_scatter x1, waiting for transfers between devices: 15.6 us -> 6.91 us  [per_device(): lax.psum_scatter(partial_value, 'tp', scatter_dimension=2, tiled=True)]
    ppermute x0 -> x3, waiting for transfers between devices: none -> 8.04 us  [per_device(): lax.ppermute(router_grad, 'ep', [(dev, dev ^ hop) for dev in range(8)])]
    all_to_all x1, waiting for transfers between devices: 0.01 us -> 6.39 us  [per_device(): lax.all_to_all(gate_send, 'ep', split_axis=1, concat_axis=1, tiled=True)]
    ppermute x0 -> x3, starting transfers between devices: none -> 4.12 us  [per_device(): lax.ppermute(router_grad, 'ep', [(dev, dev ^ hop) for dev in range(8)])]
    unnamed x30 -> x28, local copies, waits for them, and re-layouts: 9.92 us -> 9.91 us
  transfers between devices with their start and end apart: 6 -> 9, of which waited for: 4 -> 7; matrix products, arithmetic and copies ran while one was open for 17% -> 18% of each run, Pallas kernels for 0% -> 0%
where the time goes in v1:
time: 229 us; the launch traced here: 228 us
  waiting for transfers between devices  95.8 us (42%)
  matrix products  33.1 us (14%)
  starting transfers between devices  30.3 us (13%)
  local copies, waits for them, and re-layouts  30 us (13%)
  blocking collectives  17.5 us (8%)
  between operations  14.3 us (6%)
  other arithmetic  6.74 us (3%)
    all_to_all x1, waiting for transfers between devices, per_device(): lax.all_to_all(rows_send, 'ep', split_axis=1, concat_axis=1, tiled=True)  37.2 us
    all_to_all x1, waiting for transfers between devices, per_device(): lax.all_to_all(cots_send, 'ep', split_axis=1, concat_axis=1, tiled=True)  34.1 us
    psum x1, blocking collectives, per_device(): gate_sum = lax.psum(gate_term, 'tp')  11 us
    unnamed x28, local copies, waits for them, and re-layouts  9.91 us
    ppermute x3, waiting for transfers between devices, per_device(): lax.ppermute(router_grad, 'ep', [(dev, dev ^ hop) for dev in range(8)])  8.04 us
    all_to_all x1, starting transfers between devices, per_device(): lax.all_to_all(scale_send, 'ep', split_axis=1, concat_axis=1, tiled=True)  7.28 us
    reduce_scatter x1, waiting for transfers between devices, per_device(): lax.psum_scatter(partial_value, 'tp', scatter_dimension=2, tiled=True)  6.91 us
    all_gather x1, blocking collectives, per_device(): token_grad = lax.all_gather(token_grad, 'tp', axis=1, tiled=True)  6.5 us
  transfers between devices with their start and end apart: 9, of which 7 were waited for; matrix products, arithmetic and copies ran while one was open for 18% of the time, Pallas kernels for 0%

profile of v1, /device:TPU:0, one launch (start us, length us, event | category | flops | bytes accessed | tf_op | source)
XLA Modules:
  0.0 227.8 jit_solution(2855601267378167343)
XLA Ops:
  7.2 0.8 broadcast_multiply_fusion
  8.0 0.8 copy.81
  9.1 0.7 bitcast_or_fusion
  10.0 0.6 reduce-window.6
  11.0 1.4 scatter_custom_fusion
  12.7 1.3 fusion.14
  14.0 1.4 gather_fusion.5
  15.6 0.5 fusion.29
  16.5 3.2 %gather_fusion = bf16[448]{0:T(512)(128)(2,1)S(1)} fusion(bf16[257]{0:T(512)(128)(2,1)S(1)} %pad_maximum_fusion, s32[1024]{0:T(1024)S(1)} %get-tuple-element.85), kind=kCustom, calls=%fused_computation | custom fusion | bytes 3584 | tf_op jit(solution)/shard_map/gather | solution.py:74
  19.6 0.7 reshape.229
  20.3 7.3 %all-to-all-start = ((bf16[1,8,56]{2,0,1:T(2,128)(2,1)}), bf16[1,8,56]{2,0,1:T(2,128)(2,1)S(1)}, u32[]{:S(2)}, u32[]{:S(2)}) async-start(bf16[1,8,56]{2,0,1:T(2,128)(2,1)} %reshape.229), calls=%async_computation | async-start | bytes 8192 | tf_op jit(solution)/shard_map/all_to_all | solution.py:78
  27.7 3.2 %gather_fusion.2 = bf16[448,2048]{1,0:T(8,128)(2,1)} fusion(bf16[129,2048]{1,0:T(8,128)(2,1)S(1)} %concatenate.11, s32[1024]{0:T(1024)S(1)} %get-tuple-element.84), kind=kCustom, calls=%fused_computation.2 | custom fusion | bytes 3671808 | tf_op jit(solution)/shard_map/gather | solution.py:72
  30.9 3.2 %all-to-all-done = bf16[1,8,56]{2,0,1:T(2,128)(2,1)S(1)} async-done(((bf16[1,8,56]{2,0,1:T(2,128)(2,1)}), bf16[1,8,56]{2,0,1:T(2,128)(2,1)S(1)}, u32[]{:S(2)}, u32[]{:S(2)}) %all-to-all-start) | async-done | bytes 928 | tf_op jit(solution)/shard_map/all_to_all | solution.py:78
  34.0 4.3 %all-to-all-start.2 = ((bf16[1,8,56,2048]{3,2,0,1:T(8,128)(2,1)}), bf16[1,8,56,2048]{3,2,0,1:T(8,128)(2,1)}, u32[]{:S(2)}, u32[]{:S(2)}) async-start(bf16[1,8,56,2048]{3,2,0,1:T(8,128)(2,1)} %bitcast.67), calls=%async_computation.2 | async-start | bytes 3670016 | tf_op jit(solution)/shard_map/all_to_all | solution.py:76
  38.3 1.1 concatenate.10
  39.4 3.2 %gather_fusion.1 = bf16[448,2048]{1,0:T(8,128)(2,1)} fusion(bf16[129,2048]{1,0:T(8,128)(2,1)S(1)} %concatenate.10, s32[1024]{0:T(1024)S(1)} %get-tuple-element.84), kind=kCustom, calls=%fused_computation.1 | custom fusion | bytes 3671808 | tf_op jit(solution)/shard_map/gather | solution.py:73
  42.6 37.2 %all-to-all-done.2 = bf16[1,8,56,2048]{3,2,0,1:T(8,128)(2,1)} async-done(((bf16[1,8,56,2048]{3,2,0,1:T(8,128)(2,1)}), bf16[1,8,56,2048]{3,2,0,1:T(8,128)(2,1)}, u32[]{:S(2)}, u32[]{:S(2)}) %all-to-all-start.2) | async-done | bytes 1835040 | tf_op jit(solution)/shard_map/all_to_all | solution.py:76
  79.8 4.3 %all-to-all-start.1 = ((bf16[1,8,56,2048]{3,2,0,1:T(8,128)(2,1)}), bf16[1,8,56,2048]{3,2,0,1:T(8,128)(2,1)}, u32[]{:S(2)}, u32[]{:S(2)}) async-start(bf16[1,8,56,2048]{3,2,0,1:T(8,128)(2,1)} %bitcast.66), calls=%async_computation.1 | async-start | bytes 3670016 | tf_op jit(solution)/shard_map/all_to_all | solution.py:77
  84.5 4.2 %fusion.5 = f32[448,512]{1,0:T(8,128)} fusion(bf16[448,2048]{1,0:T(8,128)(2,1)} %bitcast.11, bf16[1,2048,512]{2,1,0:T(8,128)(2,1)} %param.11), kind=kOutput, calls=%fused_computation.17 | convolution fusion | flops 939524096 | bytes 4849664 | tf_op jit(solution)/shard_map/dot_general | solution.py:9
  88.7 3.5 %fusion.2 = f32[448,512]{1,0:T(8,128)} fusion(bf16[448,2048]{1,0:T(8,128)(2,1)} %bitcast.11, bf16[1,2048,512]{2,1,0:T(8,128)(2,1)S(1)} %copy-done), kind=kOutput, calls=%fused_computation.14 | convolution fusion | flops 939524096 | bytes 4849664 | tf_op jit(solution)/shard_map/dot_general | solution.py:8
  92.2 34.1 %all-to-all-done.1 = bf16[1,8,56,2048]{3,2,0,1:T(8,128)(2,1)} async-done(((bf16[1,8,56,2048]{3,2,0,1:T(8,128)(2,1)}), bf16[1,8,56,2048]{3,2,0,1:T(8,128)(2,1)}, u32[]{:S(2)}, u32[]{:S(2)}) %all-to-all-start.1) | async-done | bytes 1835040 | tf_op jit(solution)/shard_map/all_to_all | solution.py:77
  126.3 5.5 %multiply_reduce_fusion.3 = (f32[448]{0:T(512)}, bf16[448,512]{1,0:T(8,128)(2,1)}, bf16[448,512]{1,0:T(8,128)(2,1)S(1)}, bf16[448,512]{1,0:T(8,128)(2,1)S(1)}) fusion(f32[448,512]{1,0:T(8,128)} %fusion.5, f32[448,512]{1,0:T(8,128)} %fusion.2, f32[448]{0:T(512)S(1)} %reshape.164, bf16[448,2048]{1,0:T(8,128)(2,1)} %bitcast.7, bf16[1,512,2048]{2,1,0:T(8,128)(2,1)} %param.12), kind=kOutput, calls=%fused_computation.32 | convolution fusion | flops 944111168 | bytes 7147008 | tf_op jit(solution)/shard_map/dot_general | solution.py:12
  131.8 1.1 fusion
  133.0 0.4 copy-done.2
  133.4 3.0 %add_bitcast_fusion = f32[1,448,2048]{2,1,0:T(8,128)} fusion(f32[448,2048]{1,0:T(8,128)S(1)} %fusion, bf16[448,512]{1,0:T(8,128)(2,1)S(1)} %get-tuple-element.81, bf16[1,2048,512]{2,1,0:T(8,128)(2,1)S(1)} %copy-done.2), kind=kOutput, calls=%fused_computation.11 | convolution fusion | flops 940441600 | bytes 9895936 | tf_op jit(solution)/shard_map/dot_general | solution.py:34
  136.5 4.1 %convert_bitcast_fusion.2 = (bf16[1,2048,512]{1,2,0:T(8,128)(2,1)}, f32[2048]{0:T(1024)S(1)}) fusion(bf16[448,2048]{1,0:T(8,128)(2,1)} %bitcast.11, bf16[448,512]{1,0:T(8,128)(2,1)S(1)} %get-tuple-element.80), kind=kOutput, calls=%fused_computation.23 | convolution fusion | flops 942667776 | bytes 4399104 | tf_op jit(solution)/shard_map/dot_general | solution.py:24
  140.6 4.3 %convert_bitcast_fusion.1 = (bf16[1,2048,512]{1,2,0:T(8,128)(2,1)}, f32[2048]{0:T(1024)S(1)}) fusion(bf16[448,2048]{1,0:T(8,128)(2,1)} %bitcast.11, bf16[448,512]{1,0:T(8,128)(2,1)S(1)} %get-tuple-element.81), kind=kOutput, calls=%fused_computation.22 | convolution fusion | flops 942667776 | bytes 4399104 | tf_op jit(solution)/shard_map/dot_general | solution.py:27
  144.9 11.0 %all-reduce.2 = (bf16[1,448]{1,0:T(2,128)(2,1)S(1)}, f32[1,2048]{1,0:T(1,128)}, f32[1,2048]{1,0:T(1,128)}) all-reduce(f32[1,448]{1,0:T(1,128)S(1)} %bitcast.73, f32[1,2048]{1,0:T(1,128)S(1)} %bitcast.68, f32[1,2048]{1,0:T(1,128)S(1)} %bitcast.69), channel_id=1, replica_groups=mesh['ep'=8,'tp'=4] {'tp'}, use_global_device_ids=true, to_apply=%region_8.9 | all-reduce | flops 4544 | bytes 35456 | tf_op jit(solution)/shard_map/psum | solution.py:105
  155.9 0.7 reshape.230
  156.6 4.5 %all-to-all-start.4 = ((bf16[1,8,56]{2,0,1:T(2,128)(2,1)}), bf16[1,8,56]{2,0,1:T(2,128)(2,1)S(1)}, u32[]{:S(2)}, u32[]{:S(2)}) async-start(bf16[1,8,56]{2,0,1:T(2,128)(2,1)} %reshape.230), calls=%async_computation.5 | async-start | bytes 8192 | tf_op jit(solution)/shard_map/all_to_all | solution.py:110
  161.2 6.4 %all-to-all-done.4 = bf16[1,8,56]{2,0,1:T(2,128)(2,1)S(1)} async-done(((bf16[1,8,56]{2,0,1:T(2,128)(2,1)}), bf16[1,8,56]{2,0,1:T(2,128)(2,1)S(1)}, u32[]{:S(2)}, u32[]{:S(2)}) %all-to-all-start.4) | async-done | bytes 928 | tf_op jit(solution)/shard_map/all_to_all | solution.py:110
  167.7 1.9 gather_fusion.4
  169.9 6.9 %reduce-scatter.2.cloned.1.call-done = f32[1,448,512]{2,1,0:T(8,128)} async-done(((f32[1,448,2048]{2,1,0:T(8,128)}), f32[1,448,512]{2,1,0:T(8,128)}) %reduce-scatter.2.cloned.1.call-update) | async-done | bytes 917520 | tf_op jit(solution)/shard_map/reduce_scatter | solution.py:104
  176.8 2.0 convert_element_type.94
  178.8 5.5 %all-to-all-start.3 = ((bf16[1,8,56,512]{3,2,0,1:T(8,128)(2,1)}), bf16[1,8,56,512]{3,2,0,1:T(8,128)(2,1)S(1)}, u32[]{:S(2)}, u32[]{:S(2)}) async-start(bf16[1,8,56,512]{3,2,0,1:T(8,128)(2,1)} %bitcast.16), calls=%async_computation.4 | async-start | bytes 917504 | tf_op jit(solution)/shard_map/all_to_all | solution.py:109
  184.4 2.0 collective-permute-start
  186.5 4.3 %collective-permute-done = f32[512,8]{0,1:T(8,128)S(1)} collective-permute-done((f32[512,8]{0,1:T(8,128)S(1)}, f32[512,8]{0,1:T(8,128)S(1)}, u32[]{:S(2)}, u32[]{:S(2)}) %collective-permute-start) | collective-permute-done | bytes 16416 | tf_op jit(solution)/shard_map/ppermute | solution.py:130
  191.0 3.8 %collective-permute-done.1 = f32[512,8]{0,1:T(8,128)S(1)} collective-permute-done((f32[512,8]{0,1:T(8,128)S(1)}, f32[512,8]{0,1:T(8,128)S(1)}, u32[]{:S(2)}, u32[]{:S(2)}) %collective-permute-start.1) | collective-permute-done | bytes 16416 | tf_op jit(solution)/shard_map/ppermute | solution.py:130
  194.8 1.9 collective-permute-start.2
  196.6 4.9 %multiply_reduce_fusion = (f32[512]{0:T(512)}, bf16[1,512,2048]{2,1,0:T(8,128)(2,1)}) fusion(bf16[448,512]{1,0:T(8,128)(2,1)} %get-tuple-element.69, bf16[448,2048]{1,0:T(8,128)(2,1)} %bitcast.7, f32[448]{0:T(512)S(1)} %copy-done.10), kind=kOutput, calls=%fused_computation.7 | convolution fusion | flops 945421824 | bytes 4394752 | tf_op jit(solution)/shard_map/dot_general | solution.py:23
  201.6 3.9 %copy.90 = bf16[1,2048,512]{2,1,0:T(8,128)(2,1)} copy(bf16[1,2048,512]{1,2,0:T(8,128)(2,1)} %get-tuple-element.78) | data formatting | bytes 4194304
  205.5 3.9 %copy.91 = bf16[1,2048,512]{2,1,0:T(8,128)(2,1)} copy(bf16[1,2048,512]{1,2,0:T(8,128)(2,1)} %get-tuple-element.76) | data formatting | bytes 4194304
  209.4 1.2 multiply_reduce_fusion.4
  210.6 1.2 gather_fusion.3
  212.1 0.6 reduce_sum.101
  212.7 0.9 fusion.11
  213.6 6.5 %all_gather.3 = bf16[128,2048]{1,0:T(8,128)(2,1)S(1)} all-gather(bf16[128,512]{1,0:T(8,128)(2,1)S(1)} %fusion.11), channel_id=1, replica_groups=mesh['ep'=8,'tp'=4] {'tp'}, dimensions={1}, use_global_device_ids=true | all-gather | bytes 655360 | tf_op jit(solution)/shard_map/all_gather | solution.py:138
  220.1 0.8 copy.93
  (65 shorter events, 3.2 us)
Async XLA Ops:
  7.2 81.5 %copy-start = (bf16[1,2048,512]{2,1,0:T(8,128)(2,1)S(1)}, bf16[1,2048,512]{2,1,0:T(8,128)(2,1)}, u32[]{:S(2)}) copy-start(bf16[1,2048,512]{2,1,0:T(8,128)(2,1)} %param.10) | copy-start | bytes 6291460
  11.0 1.7 copy-start.6
  14.0 1.6 copy-start.3
  14.0 13.6 %copy-start.1 = (bf16[128,2048]{1,0:T(8,128)(2,1)S(1)}, bf16[128,2048]{1,0:T(8,128)(2,1)}, u32[]{:S(2)}) copy-start(bf16[128,2048]{1,0:T(8,128)(2,1)} %param.7) | copy-start | bytes 1572868
  15.6 15.2 %copy-start.4 = (f32[128]{0:T(128)}, f32[128]{0:T(128)S(1)}, u32[]{:S(2)}) copy-start(f32[128]{0:T(128)S(1)} %get-tuple-element.72) | copy-start | bytes 1540
  20.3 13.7 %all-to-all-start = ((bf16[1,8,56]{2,0,1:T(2,128)(2,1)}), bf16[1,8,56]{2,0,1:T(2,128)(2,1)S(1)}, u32[]{:S(2)}, u32[]{:S(2)}) async-start(bf16[1,8,56]{2,0,1:T(2,128)(2,1)} %reshape.229), calls=%async_computation | async-start | bytes 8192 | tf_op jit(solution)/shard_map/all_to_all | solution.py:78
  34.0 45.8 %all-to-all-start.2 = ((bf16[1,8,56,2048]{3,2,0,1:T(8,128)(2,1)}), bf16[1,8,56,2048]{3,2,0,1:T(8,128)(2,1)}, u32[]{:S(2)}, u32[]{:S(2)}) async-start(bf16[1,8,56,2048]{3,2,0,1:T(8,128)(2,1)} %bitcast.67), calls=%async_computation.2 | async-start | bytes 3670016 | tf_op jit(solution)/shard_map/all_to_all | solution.py:76
  79.8 46.5 %all-to-all-start.1 = ((bf16[1,8,56,2048]{3,2,0,1:T(8,128)(2,1)}), bf16[1,8,56,2048]{3,2,0,1:T(8,128)(2,1)}, u32[]{:S(2)}, u32[]{:S(2)}) async-start(bf16[1,8,56,2048]{3,2,0,1:T(8,128)(2,1)} %bitcast.66), calls=%async_computation.1 | async-start | bytes 3670016 | tf_op jit(solution)/shard_map/all_to_all | solution.py:77
  84.2 92.7 %reduce-scatter.2.cloned.1.call-start = ((), (), s32[]{:S(2)}) async-start(), calls=%async_computation.6 | async-start | bytes 4587520 | tf_op jit(solution)/shard_map/reduce_scatter | solution.py:104
  84.5 41.8 %copy-start.9 = (f32[448]{0:T(512)}, f32[448]{0:T(512)S(1)}, u32[]{:S(2)}) copy-start(f32[448]{0:T(512)S(1)} %reshape.164) | copy-start | bytes 5380
  131.8 1.6 copy-start.2
  140.6 4.3 %copy-start.11 = (f32[448]{0:T(512)S(1)}, f32[448]{0:T(512)}, u32[]{:S(2)}) copy-start(f32[448]{0:T(512)} %get-tuple-element.68) | copy-start | bytes 5380
  140.6 20.6 %copy-start.7 = (s32[256,1]{0,1:T(1,128)S(1)}, s32[256,1]{0,1:T(1,128)}, u32[]{:S(2)}) copy-start(s32[256,1]{0,1:T(1,128)} %copy-done.6) | copy-start | bytes 3076
  140.6 29.2 %copy-start.8 = (f32[128,2]{0,1:T(2,128)S(1)}, f32[128,2]{0,1:T(2,128)}, u32[]{:S(2)}) copy-start(f32[128,2]{0,1:T(2,128)} %get-tuple-element.71) | copy-start | bytes 3076
  140.6 29.3 %copy-start.5 = (f32[128]{0:T(128)S(1)}, f32[128]{0:T(128)}, u32[]{:S(2)}) copy-start(f32[128]{0:T(128)} %copy-done.4) | copy-start | bytes 1540
  144.9 51.7 %copy-start.10 = (f32[448]{0:T(512)S(1)}, f32[448]{0:T(512)}, u32[]{:S(2)}) copy-start(f32[448]{0:T(512)} %copy-done.9) | copy-start | bytes 5380
  156.6 11.0 %all-to-all-start.4 = ((bf16[1,8,56]{2,0,1:T(2,128)(2,1)}), bf16[1,8,56]{2,0,1:T(2,128)(2,1)S(1)}, u32[]{:S(2)}, u32[]{:S(2)}) async-start(bf16[1,8,56]{2,0,1:T(2,128)(2,1)} %reshape.230), calls=%async_computation.5 | async-start | bytes 8192 | tf_op jit(solution)/shard_map/all_to_all | solution.py:110
  178.8 31.7 %all-to-all-start.3 = ((bf16[1,8,56,512]{3,2,0,1:T(8,128)(2,1)}), bf16[1,8,56,512]{3,2,0,1:T(8,128)(2,1)S(1)}, u32[]{:S(2)}, u32[]{:S(2)}) async-start(bf16[1,8,56,512]{3,2,0,1:T(8,128)(2,1)} %bitcast.16), calls=%async_computation.4 | async-start | bytes 917504 | tf_op jit(solution)/shard_map/all_to_all | solution.py:109
  184.4 6.3 %collective-permute-start = (f32[512,8]{0,1:T(8,128)S(1)}, f32[512,8]{0,1:T(8,128)S(1)}, u32[]{:S(2)}, u32[]{:S(2)}) collective-permute-start(f32[512,8]{0,1:T(8,128)S(1)} %fusion.15), channel_id=1, source_target_pairs={{0,4},{4,0},{8,12},{12,8},{16,20},{20,16},{24,28},{28,24},{1,5},{5... | collective-permute-start | bytes 49160 | tf_op jit(solution)/shard_map/ppermute | solution.py:130
  190.7 4.0 %collective-permute-start.1 = (f32[512,8]{0,1:T(8,128)S(1)}, f32[512,8]{0,1:T(8,128)S(1)}, u32[]{:S(2)}, u32[]{:S(2)}) collective-permute-start(f32[512,8]{0,1:T(8,128)S(1)} %add.109), channel_id=1, source_target_pairs={{0,8},{4,12},{8,0},{12,4},{16,24},{20,28},{24,16},{28,20},{1,9},{5... | collective-permute-start | bytes 49160 | tf_op jit(solution)/shard_map/ppermute | solution.py:130
  194.8 14.6 %collective-permute-start.2 = (f32[512,8]{0,1:T(8,128)S(1)}, f32[512,8]{0,1:T(8,128)S(1)}, u32[]{:S(2)}, u32[]{:S(2)}) collective-permute-start(f32[512,8]{0,1:T(8,128)S(1)} %add.110), channel_id=1, source_target_pairs={{0,16},{4,20},{8,24},{12,28},{16,0},{20,4},{24,8},{28,12},{1,17},{... | collective-permute-start | bytes 49160 | tf_op jit(solution)/shard_map/ppermute | solution.py:130
Sparse Core Ops, SparseCore 0:
  136.6 40.1 reduce-scatter.1
